TPU v7x, 512 devices: a 4x2x32 block of a 4x8x32 slice. The times are simulated.
512 devices in a mesh: grp: 2 (over y), fs: 32 (over z), tp: 8 (over x, core).
Axes of the slice: x: 4, y: 2, z: 32, core: 2. Of those that a mesh axis runs over, the one named last changes fastest.
The devices are a block of a 4x8x32 slice.
Arguments:
- tokens: bfloat16 [16384, 2048], P(('grp', 'fs')), parts along dimension 0, may hold values from -6 to 6
- norm_gain: float32 [2048], P('fs'), may hold values from 0.1 to 1.9
- gate_master: float32 [32, 2048, 1024], P(None, 'fs', 'tp'), may hold values from -0.125 to 0.125
- up_master: float32 [32, 2048, 1024], P(None, 'fs', 'tp'), may hold values from -0.125 to 0.125
- chosen: int32 [16384, 2], P(('grp', 'fs')), parts along dimension 0, may hold values from 0 to 31, all different within a row; in each aligned block of 256 rows (0 to 255, 256 to 511, ...) at most 32 rows name the same one
- affinity: float32 [16384, 2], P(('grp', 'fs')), parts along dimension 0, may hold values from 0.05 to 1
Outputs:
- gate_served: bfloat16 [64, 2048, 1024], P(('grp', 'fs'), None, 'tp'), parts along dimension 0
- up_served: bfloat16 [64, 2048, 1024], P(('grp', 'fs'), None, 'tp'), parts along dimension 0
- hidden: bfloat16 [16384, 2, 1024], P(('grp', 'fs'), None, 'tp'), parts along dimension 0
There are 2 independent parts, one for each index of `grp`. A program takes and returns all parts, laid end to end along the dimension named above; an argument that names none is the same for every part. Nothing has to cross between parts.
Inputs may be any that keep to these rules, and one draw needn't show every extreme that they name: Among the rows of one index of fs (256 tokens, all their choices) no expert is chosen more than 32 times, a bound that some block reaches; the choices of one token differ.
All inputs are finite; a program needn't handle non-finite values.
Results may differ from a plain program's by a relative error of at most 0.023.
Values may be sent and summed in bfloat16 or wider, within the bound.
No kernel may reach another device: no remote copies, remote signals or barrier semaphores. Data moves between devices by JAX's collectives and lax.ppermute only.
A program may use at most 64 MiB of HBM per device.

v0:
```python
import jax
import jax.numpy as jnp
from jax import lax
from jax.sharding import PartitionSpec as P


def side_by_side(arrays, axis, split_dim, concat_dim, along):
    ends, at = ([], 0)
    for a in arrays[:-1]:
        at += a.shape[along]
        ends.append(at)
    both = jnp.concatenate(arrays, axis=along)
    return tuple(
        jnp.split(
            lax.all_to_all(both, axis, split_axis=split_dim, concat_axis=concat_dim, tiled=True),
            ends,
            axis=along,
        )
    )


def on_device(tokens, norm_gain, gate_master, up_master, chosen, affinity):
    folded_gate = (gate_master * norm_gain[None, :, None]).astype(jnp.bfloat16)
    folded_up = (up_master * norm_gain[None, :, None]).astype(jnp.bfloat16)
    new_gate, new_up = side_by_side((folded_gate, folded_up), "fs", 0, 1, 2)
    experts_all = gate_master.shape[0]
    tok_rows, width = tokens.shape
    top = chosen.shape[1]
    capacity = tok_rows * top * 2 // experts_all
    local = new_gate.shape[0]
    xfloat = tokens.astype(jnp.float32)
    scale = lax.rsqrt(jnp.mean(xfloat * xfloat, axis=-1) + 1e-06)
    share = affinity / jnp.sum(affinity, axis=-1, keepdims=True)
    flat_e = chosen.reshape(-1)
    onehot = (flat_e[:, None] == jnp.arange(experts_all, dtype=jnp.int32)[None, :]).astype(
        jnp.int32
    )
    slot = jnp.sum((jnp.cumsum(onehot, axis=0) - onehot) * onehot, axis=1)
    target = flat_e * capacity + slot
    owner = jnp.repeat(jnp.arange(tok_rows, dtype=jnp.int32), top)
    total = experts_all * capacity
    scale_buf = (
        jnp.zeros((total,), jnp.float32).at[target].set(scale[owner]).reshape(experts_all, capacity)
    )
    share_buf = (
        jnp.zeros((total,), jnp.float32)
        .at[target]
        .set(share.reshape(-1))
        .reshape(experts_all, capacity)
    )
    narrow = width // lax.axis_size("tp")
    own_cols = lax.dynamic_slice_in_dim(tokens, lax.axis_index("tp") * narrow, narrow, 1)
    row_buf = jnp.zeros((total, narrow), jnp.bfloat16).at[target].set(own_cols[owner])
    row_buf = row_buf.reshape(experts_all, capacity, narrow)
    got_rows, got_scale, got_share = (
        lax.all_to_all(row_buf, "fs", split_axis=0, concat_axis=0, tiled=True),
        lax.all_to_all(
            scale_buf.astype(jnp.bfloat16), "fs", split_axis=0, concat_axis=0, tiled=True
        ).astype(scale_buf.dtype),
        lax.all_to_all(
            share_buf.astype(jnp.bfloat16), "fs", split_axis=0, concat_axis=0, tiled=True
        ).astype(share_buf.dtype),
    )
    sources = got_rows.shape[0] // local
    got_rows = got_rows.reshape(sources, local, capacity, narrow)
    piece = lax.all_gather(got_rows, "tp", axis=3, tiled=True)
    more_gate = jnp.einsum("secd,edf->secf", piece, new_gate, preferred_element_type=jnp.float32)
    more_up = jnp.einsum("secd,edf->secf", piece, new_up, preferred_element_type=jnp.float32)
    gate = more_gate
    up = more_up
    factor = got_scale.reshape(sources, local, capacity)[..., None]
    weight = got_share.reshape(sources, local, capacity)[..., None]
    gate = gate * factor
    up = up * factor
    hidden_rows = (weight * jax.nn.silu(gate) * up).astype(jnp.bfloat16)
    hidden_rows = hidden_rows.reshape(sources * local, capacity, hidden_rows.shape[3])
    back = lax.all_to_all(hidden_rows, "fs", split_axis=0, concat_axis=0, tiled=True)
    picked = back.reshape(total, back.shape[2])[target].reshape(tok_rows, top, back.shape[2])
    return (new_gate, new_up, picked)


def solution(mesh):
    return jax.shard_map(
        on_device,
        mesh=mesh,
        in_specs=(
            P(("grp", "fs"), None),
            P("fs"),
            P(None, "fs", "tp"),
            P(None, "fs", "tp"),
            P(("grp", "fs"), None),
            P(("grp", "fs"), None),
        ),
        out_specs=(
            P(("grp", "fs"), None, "tp"),
            P(("grp", "fs"), None, "tp"),
            P(("grp", "fs"), None, "tp"),
        ),
        check_vma=False,
    )
```

profile of v0, /device:TPU:46, one launch (start us, length us, event | category | flops | bytes accessed | tf_op | source)
XLA Modules:
  0.0 353.4 jit_solution(17771561257610576837)
XLA Ops:
  7.2 0.8 broadcast_multiply_fusion
  8.1 0.8 copy.20
  8.9 0.1 eq.25
  9.3 0.1 mul.79
  9.5 1.2 reduce-window.6
  10.6 0.2 slice_reduce_fusion
  11.1 1.5 multiply_reduce_fusion
  12.7 3.5 gather_fusion
  16.2 2.4 scatter_custom_fusion.2
  18.7 0.7 convert_element_type.82
  19.4 45.8 %all-to-all-start.3 = ((bf16[32,1,32]{2,1,0:T(2,128)(2,1)}), bf16[32,1,32]{2,1,0:T(2,128)(2,1)S(1)}, u32[]{:S(2)}, u32[]{:S(2)}) async-start(bf16[32,1,32]{2,1,0:T(2,128)(2,1)} %convert_element_type.82), calls=%async_computation.3 | async-start | bytes 32768 | tf_op jit(solution)/shard_map/all_to_all | solution.py:57
  65.3 0.1 reshape.207
  65.5 2.4 scatter_custom_fusion
  67.9 0.7 convert_element_type.81
  68.6 18.1 %all-to-all-done.3 = bf16[32,1,32]{2,1,0:T(2,128)(2,1)S(1)} async-done(((bf16[32,1,32]{2,1,0:T(2,128)(2,1)}), bf16[32,1,32]{2,1,0:T(2,128)(2,1)S(1)}, u32[]{:S(2)}, u32[]{:S(2)}) %all-to-all-start.3) | async-done | bytes 2080 | tf_op jit(solution)/shard_map/all_to_all | solution.py:57
  86.8 4.7 %all-to-all-start.1 = ((bf16[32,1,32]{2,1,0:T(2,128)(2,1)}), bf16[32,1,32]{2,1,0:T(2,128)(2,1)S(1)}, u32[]{:S(2)}, u32[]{:S(2)}) async-start(bf16[32,1,32]{2,1,0:T(2,128)(2,1)} %convert_element_type.81), calls=%async_computation.1 | async-start | bytes 32768 | tf_op jit(solution)/shard_map/all_to_all | solution.py:60
  91.5 0.9 constant_dynamic-slice_fusion
  92.4 4.6 %scatter_custom_fusion.1 = bf16[1024,256]{1,0:T(8,128)(2,1)} fusion(s32[512]{0:T(512)S(1)} %bitcast.76, bf16[256,256]{1,0:T(8,128)(2,1)S(1)} %constant_dynamic-slice_fusion, s32[1024]{0:T(1024)S(1)} %pad_clamp_fusion.1, bf16[]{:T(256)} %constant.6.clone.1), kind=kCustom, calls=%fused_computation.21 | custom fusion | bytes 524290 | tf_op jit(solution)/shard_map/scatter | solution.py:53
  97.0 15.9 %all-to-all-done.1 = bf16[32,1,32]{2,1,0:T(2,128)(2,1)S(1)} async-done(((bf16[32,1,32]{2,1,0:T(2,128)(2,1)}), bf16[32,1,32]{2,1,0:T(2,128)(2,1)S(1)}, u32[]{:S(2)}, u32[]{:S(2)}) %all-to-all-start.1) | async-done | bytes 2080 | tf_op jit(solution)/shard_map/all_to_all | solution.py:60
  112.9 6.1 %all-to-all-start.2 = ((bf16[32,32,256]{2,1,0:T(8,128)(2,1)}), bf16[32,32,256]{2,1,0:T(8,128)(2,1)S(1)}, u32[]{:S(2)}, u32[]{:S(2)}) async-start(bf16[32,32,256]{2,1,0:T(8,128)(2,1)} %bitcast.8), calls=%async_computation.2 | async-start | bytes 1048576 | tf_op jit(solution)/shard_map/all_to_all | solution.py:56
  119.0 0.3 multiply_convert_fusion.1
  119.4 1.1 pad_maximum_fusion
  120.5 61.3 %all-to-all-done.2 = bf16[32,32,256]{2,1,0:T(8,128)(2,1)S(1)} async-done(((bf16[32,32,256]{2,1,0:T(8,128)(2,1)}), bf16[32,32,256]{2,1,0:T(8,128)(2,1)S(1)}, u32[]{:S(2)}, u32[]{:S(2)}) %all-to-all-start.2) | async-done | bytes 524320 | tf_op jit(solution)/shard_map/all_to_all | solution.py:56
  181.8 4.8 %all-to-all-start = ((bf16[32,64,256]{2,1,0:T(8,128)(2,1)}), bf16[32,64,256]{2,1,0:T(8,128)(2,1)S(1)}, u32[]{:S(2)}, u32[]{:S(2)}) async-start(bf16[32,64,256]{2,1,0:T(8,128)(2,1)} %pad_maximum_fusion), calls=%async_computation | async-start | bytes 2097152 | tf_op jit(solution)/shard_map/all_to_all | solution.py:15
  186.7 0.2 all-gather.3.cloned.1.call-start
  187.0 0.5 all-gather.3.cloned.1.call-update
  187.5 105.8 %all-to-all-done = bf16[32,64,256]{2,1,0:T(8,128)(2,1)S(1)} async-done(((bf16[32,64,256]{2,1,0:T(8,128)(2,1)}), bf16[32,64,256]{2,1,0:T(8,128)(2,1)S(1)}, u32[]{:S(2)}, u32[]{:S(2)}) %all-to-all-start) | async-done | bytes 1048608 | tf_op jit(solution)/shard_map/all_to_all | solution.py:15
  293.5 3.8 %fusion.3 = f32[32,1,32,128]{3,2,0,1:T(8,128)S(1)} fusion(bf16[32,32,2048]{2,1,0:T(8,128)(2,1)} %all-gather.3.cloned.1.call-done, bf16[1,2048,128]{2,1,0:T(8,128)(2,1)S(1)} %get-tuple-element.4, f32[32,32]{1,0:T(8,128)S(1)} %bitcast.71), kind=kOutput, calls=%fused_computation.12 | convolution fusion | flops 537001984 | bytes 5246976 | tf_op jit(solution)/shard_map/secd,edf->secf/dot_general | solution.py:67
  297.3 2.0 fusion.6
  299.3 4.8 %all-to-all-start.4 = ((bf16[32,32,128]{2,1,0:T(8,128)(2,1)}), bf16[32,32,128]{2,1,0:T(8,128)(2,1)S(1)}, u32[]{:S(2)}, u32[]{:S(2)}) async-start(bf16[32,32,128]{2,1,0:T(8,128)(2,1)} %fusion.6), calls=%async_computation.4 | async-start | bytes 524288 | tf_op jit(solution)/shard_map/all_to_all | solution.py:77
  304.1 40.5 %all-to-all-done.4 = bf16[32,32,128]{2,1,0:T(8,128)(2,1)S(1)} async-done(((bf16[32,32,128]{2,1,0:T(8,128)(2,1)}), bf16[32,32,128]{2,1,0:T(8,128)(2,1)S(1)}, u32[]{:S(2)}, u32[]{:S(2)}) %all-to-all-start.4) | async-done | bytes 262176 | tf_op jit(solution)/shard_map/all_to_all | solution.py:77
  344.6 1.9 gather_fusion.1
  (38 shorter events, 0.9 us)
Async XLA Ops:
  7.2 58.0 %copy-start.5 = (f32[256,2]{0,1:T(2,128)S(1)}, f32[256,2]{0,1:T(2,128)}, u32[]{:S(2)}) copy-start(f32[256,2]{0,1:T(2,128)} %param.11) | copy-start | bytes 6148
  7.2 111.8 %copy-start.1 = (f32[32,64,128]{2,1,0:T(8,128)S(1)}, f32[32,64,128]{2,1,0:T(8,128)}, u32[]{:S(2)}) copy-start(f32[32,64,128]{2,1,0:T(8,128)} %param.8) | copy-start | bytes 3145732
  7.2 111.8 %copy-start.6 = (f32[64]{0:T(128)S(1)}, f32[64]{0:T(128)}, u32[]{:S(2)}) copy-start(f32[64]{0:T(128)} %param.7) | copy-start | bytes 772
  7.2 111.8 %copy-start.2 = (f32[32,64,128]{2,1,0:T(8,128)S(1)}, f32[32,64,128]{2,1,0:T(8,128)}, u32[]{:S(2)}) copy-start(f32[32,64,128]{2,1,0:T(8,128)} %param.9) | copy-start | bytes 3145732
  19.4 67.4 %all-to-all-start.3 = ((bf16[32,1,32]{2,1,0:T(2,128)(2,1)}), bf16[32,1,32]{2,1,0:T(2,128)(2,1)S(1)}, u32[]{:S(2)}, u32[]{:S(2)}) async-start(bf16[32,1,32]{2,1,0:T(2,128)(2,1)} %convert_element_type.82), calls=%async_computation.3 | async-start | bytes 32768 | tf_op jit(solution)/shard_map/all_to_all | solution.py:57
  86.8 26.1 %all-to-all-start.1 = ((bf16[32,1,32]{2,1,0:T(2,128)(2,1)}), bf16[32,1,32]{2,1,0:T(2,128)(2,1)S(1)}, u32[]{:S(2)}, u32[]{:S(2)}) async-start(bf16[32,1,32]{2,1,0:T(2,128)(2,1)} %convert_element_type.81), calls=%async_computation.1 | async-start | bytes 32768 | tf_op jit(solution)/shard_map/all_to_all | solution.py:60
  112.9 69.0 %all-to-all-start.2 = ((bf16[32,32,256]{2,1,0:T(8,128)(2,1)}), bf16[32,32,256]{2,1,0:T(8,128)(2,1)S(1)}, u32[]{:S(2)}, u32[]{:S(2)}) async-start(bf16[32,32,256]{2,1,0:T(8,128)(2,1)} %bitcast.8), calls=%async_computation.2 | async-start | bytes 1048576 | tf_op jit(solution)/shard_map/all_to_all | solution.py:56
  181.8 5.1 %copy-start = (bf16[32,32,256]{2,1,0:T(8,128)(2,1)}, bf16[32,32,256]{2,1,0:T(8,128)(2,1)S(1)}, u32[]{:S(2)}) copy-start(bf16[32,32,256]{2,1,0:T(8,128)(2,1)S(1)} %all-to-all-done.2) | copy-start | bytes 1572868
  181.8 111.5 %all-to-all-start = ((bf16[32,64,256]{2,1,0:T(8,128)(2,1)}), bf16[32,64,256]{2,1,0:T(8,128)(2,1)S(1)}, u32[]{:S(2)}, u32[]{:S(2)}) async-start(bf16[32,64,256]{2,1,0:T(8,128)(2,1)} %pad_maximum_fusion), calls=%async_computation | async-start | bytes 2097152 | tf_op jit(solution)/shard_map/all_to_all | solution.py:15
  186.7 106.7 %all-gather.3.cloned.1.call-start = ((), (), s32[]{:S(2)}) async-start(), calls=%async_computation.5 | async-start | bytes 4718592 | tf_op jit(solution)/shard_map/all_gather | solution.py:66
  293.4 3.9 %copy-start.4 = (bf16[1,2048,128]{2,1,0:T(8,128)(2,1)}, bf16[1,2048,128]{2,1,0:T(8,128)(2,1)S(1)}, u32[]{:S(2)}) copy-start(bf16[1,2048,128]{2,1,0:T(8,128)(2,1)S(1)} %get-tuple-element.4) | copy-start | bytes 1572868
  293.4 3.9 %copy-start.3 = (bf16[1,2048,128]{2,1,0:T(8,128)(2,1)}, bf16[1,2048,128]{2,1,0:T(8,128)(2,1)S(1)}, u32[]{:S(2)}) copy-start(bf16[1,2048,128]{2,1,0:T(8,128)(2,1)S(1)} %get-tuple-element.3) | copy-start | bytes 1572868
  293.4 3.9 %copy-start.7 = (bf16[32,32,2048]{2,1,0:T(8,128)(2,1)S(1)}, bf16[32,32,2048]{2,1,0:T(8,128)(2,1)}, u32[]{:S(2)}) copy-start(bf16[32,32,2048]{2,1,0:T(8,128)(2,1)} %all-gather.3.cloned.1.call-done) | copy-start | bytes 12582916
  299.3 45.3 %all-to-all-start.4 = ((bf16[32,32,128]{2,1,0:T(8,128)(2,1)}), bf16[32,32,128]{2,1,0:T(8,128)(2,1)S(1)}, u32[]{:S(2)}, u32[]{:S(2)}) async-start(bf16[32,32,128]{2,1,0:T(8,128)(2,1)} %fusion.6), calls=%async_computation.4 | async-start | bytes 524288 | tf_op jit(solution)/shard_map/all_to_all | solution.py:77
Sparse Core Ops, SparseCore 0:
  189.7 50.9 all-gather.2
where the time goes:
time: 354 us; the launch traced here: 353 us
  waiting for transfers between devices  242 us (68%)
  starting transfers between devices  66.5 us (19%)
  local copies, waits for them, and re-layouts  19.3 us (5%)
  between operations  14.4 us (4%)
  matrix products  5.78 us (2%)
  other arithmetic  5.22 us (1%)
    all_to_all x1, waiting for transfers between devices, side_by_side(): lax.all_to_all(both, axis, split_axis=split_dim, concat_axis=concat_dim,...  106 us
    all_to_all x1, waiting for transfers between devices, on_device(): lax.all_to_all(row_buf, 'fs', split_axis=0, concat_axis=0, tiled=True)  61.3 us
    all_to_all x1, starting transfers between devices, on_device(): lax.all_to_all(scale_buf.astype(jnp.bfloat16), 'fs', split_axis=0, concat...  45.8 us
    all_to_all x1, waiting for transfers between devices, on_device(): lax.all_to_all(hidden_rows, 'fs', split_axis=0, concat_axis=0, tiled=True)  40.5 us
    all_to_all x1, waiting for transfers between devices, on_device(): lax.all_to_all(scale_buf.astype(jnp.bfloat16), 'fs', split_axis=0, concat...  18.1 us
    all_to_all x1, waiting for transfers between devices, on_device(): lax.all_to_all(share_buf.astype(jnp.bfloat16), 'fs', split_axis=0, concat...  15.9 us
  transfers between devices with their start and end apart: 6, of which 5 were waited for; matrix products, arithmetic and copies ran while one was open for 3% of the time, Pallas kernels for 0%

commit v1 on v0

v1 whole, which is shorter than its diff:
```python
import functools
import jax
import jax.numpy as jnp
from jax import lax
from jax.experimental import pallas as pl
from jax.experimental.pallas import tpu as pltpu
from jax.sharding import PartitionSpec as P

F32 = jnp.float32
BF16 = jnp.bfloat16


def iota(shape, dim):
    return lax.broadcasted_iota(jnp.int32, shape, dim)


def dot(a, b, dims=(((1,), (0,)), ((), ()))):
    return lax.dot_general(a, b, dims, preferred_element_type=F32)


def pack_kernel(tokens, chosen, rows, *, experts, capacity, narrow):
    n, width = tokens.shape
    x = tokens[...].astype(F32)
    scale = lax.rsqrt(jnp.sum(x * x, axis=-1, keepdims=True) / width + 1e-06)
    at = pl.multiple_of(lax.axis_index("tp") * narrow, narrow)
    own = (tokens[:, pl.ds(at, narrow)].astype(F32) * scale).astype(BF16)
    eye = (iota((n, n), 0) == iota((n, n), 1)).astype(F32).astype(BF16)
    before = (iota((n, n), 0) < iota((n, n), 1)).astype(F32).astype(BF16)
    choice = dot(chosen[...].astype(F32).astype(BF16), eye, (((0,), (0,)), ((), ())))
    named = jnp.zeros((experts, n), F32)
    expert = iota((experts, n), 0).astype(F32)
    for k in range(chosen.shape[1]):
        named = named + (choice[k : k + 1, :] == expert).astype(F32)
    slot = dot(named.astype(BF16), before)
    slot = jnp.where(named > 0, slot, -1.0)
    pick = slot[:, None, :] == iota((experts, capacity, n), 1).astype(F32)
    pick = pick.astype(F32).reshape(experts * capacity, n).astype(BF16)
    rows[...] = dot(pick, own).astype(BF16)


def expert_kernel(parts, rows, gate, up, hidden, *, groups):
    count, sources, piece, both = parts.shape
    half = both // 2
    mine = lax.axis_index("grp")
    for q in range(count):
        at = pl.multiple_of((mine ^ q) * piece, piece)
        gate[:, pl.ds(at, piece), :] = parts[q, :, :, :half]
        up[:, pl.ds(at, piece), :] = parts[q, :, :, half:]
    slices, _, narrow = rows.shape
    block = sources * piece * count // slices
    per = gate.shape[0] // slices
    a = None
    for k in range(slices):
        w = jnp.concatenate(
            [
                gate[k * per : (k + 1) * per].reshape(block, half),
                up[k * per : (k + 1) * per].reshape(block, half),
            ],
            axis=1,
        )
        d = dot(rows[k], w)
        a = d if a is None else a + d
    g = a[:, :half]
    hidden[...] = (g / (1.0 + jnp.exp(-g)) * a[:, half:]).astype(BF16)


def pick_kernel(back, chosen, affinity, out, *, experts, capacity):
    n, top = chosen.shape
    total = back.shape[0]
    c = chosen[...]
    lane = iota((n, experts), 1)
    hot = [(c[:, k : k + 1] == lane).astype(F32) for k in range(top)]
    named = functools.reduce(jnp.add, hot)
    before = (iota((n, n), 1) < iota((n, n), 0)).astype(F32).astype(BF16)
    slot = dot(before, named.astype(BF16))
    a = affinity[...]
    share = a / jnp.sum(a, axis=-1, keepdims=True)
    slots = iota((n, total), 1)
    for k in range(top):
        at = jnp.sum(hot[k] * slot, axis=1, keepdims=True).astype(jnp.int32)
        at = at + c[:, k : k + 1] * capacity
        take = (slots == at).astype(F32).astype(BF16)
        out[:, k, :] = (dot(take, back[...]) * share[:, k : k + 1]).astype(BF16)


def on_device(tokens, norm_gain, gate_master, up_master, chosen, affinity):
    groups, sources, slices = (lax.axis_size(a) for a in ("grp", "fs", "tp"))
    experts, block, half = gate_master.shape
    n, width = tokens.shape
    top = chosen.shape[1]
    capacity = n * top * 2 // experts
    narrow = width // slices
    piece = block // groups
    vmem = pl.BlockSpec(memory_space=pltpu.VMEM)

    rows = pl.pallas_call(
        functools.partial(pack_kernel, experts=experts, capacity=capacity, narrow=narrow),
        out_shape=jax.ShapeDtypeStruct((experts * capacity, narrow), BF16),
        in_specs=[vmem, vmem],
        out_specs=vmem,
        name="pack",
    )(tokens, chosen)
    rows = lax.all_to_all(
        rows.reshape(experts, capacity, narrow), "fs", split_axis=0, concat_axis=0, tiled=True
    )
    rows = rows.reshape(experts * capacity, narrow)

    at = lax.axis_index("grp") * piece
    gain = lax.dynamic_slice_in_dim(norm_gain, at, piece, 0)[None, :, None]
    folded = jnp.concatenate(
        [
            (lax.dynamic_slice_in_dim(m, at, piece, 1) * gain).astype(BF16)
            for m in (gate_master, up_master)
        ],
        axis=2,
    )
    folded, rows = lax.optimization_barrier((folded, rows))
    every = lax.all_gather(rows, "tp", axis=0, tiled=False)
    got = lax.all_to_all(folded, "fs", split_axis=0, concat_axis=0, tiled=True)[None]
    step = 1
    while step < groups:
        swap = [(i, i ^ step) for i in range(groups)]
        got = jnp.concatenate([got, lax.ppermute(got, "grp", swap)], axis=0)
        step *= 2

    gate, up, hidden = pl.pallas_call(
        functools.partial(expert_kernel, groups=groups),
        out_shape=(
            jax.ShapeDtypeStruct((sources, block, half), BF16),
            jax.ShapeDtypeStruct((sources, block, half), BF16),
            jax.ShapeDtypeStruct((experts * capacity, half), BF16),
        ),
        in_specs=[vmem, vmem],
        out_specs=(vmem, vmem, vmem),
        name="experts",
    )(got, every)
    back = lax.all_to_all(
        hidden.reshape(experts, capacity, half), "fs", split_axis=0, concat_axis=0, tiled=True
    )
    out = pl.pallas_call(
        functools.partial(pick_kernel, experts=experts, capacity=capacity),
        out_shape=jax.ShapeDtypeStruct((n, top, half), BF16),
        in_specs=[vmem, vmem, vmem],
        out_specs=vmem,
        name="pick",
    )(back.reshape(experts * capacity, half), chosen, affinity)
    return (
        gate.reshape(1, sources * block, half),
        up.reshape(1, sources * block, half),
        out,
    )


def solution(mesh):
    return jax.shard_map(
        on_device,
        mesh=mesh,
        in_specs=(
            P(("grp", "fs"), None),
            P("fs"),
            P(None, "fs", "tp"),
            P(None, "fs", "tp"),
            P(("grp", "fs"), None),
            P(("grp", "fs"), None),
        ),
        out_specs=(
            P(("grp", "fs"), None, "tp"),
            P(("grp", "fs"), None, "tp"),
            P(("grp", "fs"), None, "tp"),
        ),
        check_vma=False,
    )
```

time: 354 us -> 267 us (0.75)
  the two profiles are of different devices: /device:TPU:46 before, /device:TPU:34 now
where the time goes in v1:
time: 267 us
  waiting for transfers between devices  112 us (42%)
  blocking collectives  67.9 us (25%)
  starting transfers between devices  55.9 us (21%)
  between operations  14.1 us (5%)
  Pallas kernels  10.3 us (4%)
  local copies, waits for them, and re-layouts  4.52 us (2%)
    all_to_all x1, blocking collectives, on_device(): lax.all_to_all(folded, 'fs', split_axis=0, concat_axis=0, tiled=True)[None]  67.9 us
    all_to_all x1, waiting for transfers between devices, on_device(): lax.all_to_all(rows.reshape(experts, capacity, narrow), 'fs', split_axis=...  62.1 us
    all_to_all x1, starting transfers between devices, on_device(): lax.all_to_all(rows.reshape(experts, capacity, narrow), 'fs', split_axis=...  45.8 us
    all_to_all x1, waiting for transfers between devices, on_device(): lax.all_to_all(hidden.reshape(experts, capacity, half), 'fs', split_axis=...  40.6 us
    ppermute x1, waiting for transfers between devices, on_device(): got = jnp.concatenate([got, lax.ppermute(got, 'grp', swap)], axis=0)  8.97 us
    all_to_all x1, starting transfers between devices, on_device(): lax.all_to_all(hidden.reshape(experts, capacity, half), 'fs', split_axis=...  5.88 us
  transfers between devices with their start and end apart: 4, of which 3 were waited for; matrix products, arithmetic and copies ran while one was open for 2% of the time, Pallas kernels for 0%

profile of v1, /device:TPU:34, one launch (start us, length us, event | category | flops | bytes accessed | tf_op | source)
XLA Modules:
  0.0 267.0 jit_solution(17874191709288293930)
XLA Ops:
  7.2 1.5 copy.9.chosen
  8.7 2.7 %pack.1 = bf16[1024,256]{1,0:T(8,128)(2,1)} custom-call(bf16[256,2048]{1,0:T(8,128)(2,1)} %tokens.1, s32[256,2]{1,0:T(8,128)} %copy.9.chosen), custom_call_target="tpu_custom_call" | custom-call | tf_op jit(solution)/shard_map/pack/pallas_call | solution.py:96
  11.3 45.8 %all-to-all-start = ((bf16[32,32,256]{2,1,0:T(8,128)(2,1)}), bf16[32,32,256]{2,1,0:T(8,128)(2,1)S(1)}, u32[]{:S(2)}, u32[]{:S(2)}) async-start(bf16[32,32,256]{2,1,0:T(8,128)(2,1)} %bitcast.10), calls=%async_computation | async-start | bytes 1048576 | tf_op jit(solution)/shard_map/all_to_all | solution.py:103
  57.1 0.1 all-gather.3.cloned.1.call-start
  57.2 0.7 dynamic_slice.10
  57.9 1.4 multiply_convert_fusion.1
  59.3 0.1 pad_maximum_fusion.1
  59.4 62.1 %all-to-all-done = bf16[32,32,256]{2,1,0:T(8,128)(2,1)S(1)} async-done(((bf16[32,32,256]{2,1,0:T(8,128)(2,1)}), bf16[32,32,256]{2,1,0:T(8,128)(2,1)S(1)}, u32[]{:S(2)}, u32[]{:S(2)}) %all-to-all-start) | async-done | bytes 524320 | tf_op jit(solution)/shard_map/all_to_all | solution.py:103
  121.5 0.0 copy-start
  121.5 0.8 copy-done
  122.3 0.1 all-gather.3.cloned.1.call-update
  122.4 67.9 %all_to_all.15 = bf16[32,32,256]{2,1,0:T(8,128)(2,1)S(1)} all-to-all(bf16[32,32,256]{2,1,0:T(8,128)(2,1)S(1)} %pad_maximum_fusion.1), channel_id=1, replica_groups=mesh['grp'=2,'fs'=32,'tp'=8] {'fs'}, dimensions={0} | all-to-all | bytes 1048576 | tf_op jit(solution)/shard_map/all_to_all | solution.py:119
  190.3 0.0 copy-start.2
  190.3 4.2 %collective-permute-start = (bf16[1,32,32,256]{3,2,1,0:T(8,128)(2,1)S(1)}, bf16[1,32,32,256]{3,2,1,0:T(8,128)(2,1)S(1)}, u32[]{:S(2)}, u32[]{:S(2)}) collective-permute-start(bf16[1,32,32,256]{3,2,1,0:T(8,128)(2,1)S(1)} %bitcast.11), channel_id=1, source_target_pairs={{0,256},{256,0},{1,257},{257,1},{2,258},{258,2},{3,259},{259,3},{4... | collective-permute-start | bytes 1572872 | tf_op jit(solution)/shard_map/ppermute | solution.py:123
  194.5 9.0 %collective-permute-done = bf16[1,32,32,256]{3,2,1,0:T(8,128)(2,1)S(1)} collective-permute-done((bf16[1,32,32,256]{3,2,1,0:T(8,128)(2,1)S(1)}, bf16[1,32,32,256]{3,2,1,0:T(8,128)(2,1)S(1)}, u32[]{:S(2)}, u32[]{:S(2)}) %collective-permute-start) | collective-permute-done | bytes 524320 | tf_op jit(solution)/shard_map/ppermute | solution.py:123
  203.5 1.1 pad_maximum_fusion.parts
  204.5 0.0 all-gather.3.cloned.1.call-done
  204.5 4.7 %experts.1 = (bf16[32,64,128]{2,1,0:T(8,128)(2,1)}, bf16[32,64,128]{2,1,0:T(8,128)(2,1)}, bf16[1024,128]{1,0:T(8,128)(2,1)}) custom-call(bf16[2,32,32,256]{3,2,1,0:T(8,128)(2,1)} %pad_maximum_fusion.parts, bf16[8,1024,256]{2,1,0:T(8,128)(2,1)} %bitcast.8), custom_call_target="tpu_custom_call" | custom-call | tf_op jit(solution)/shard_map/experts/pallas_call | solution.py:126
  209.2 5.9 %all-to-all-start.2 = ((bf16[32,32,128]{2,1,0:T(8,128)(2,1)}), bf16[32,32,128]{2,1,0:T(8,128)(2,1)S(1)}, u32[]{:S(2)}, u32[]{:S(2)}) async-start(bf16[32,32,128]{2,1,0:T(8,128)(2,1)} %bitcast.14), calls=%async_computation.2 | async-start | bytes 524288 | tf_op jit(solution)/shard_map/all_to_all | solution.py:137
  215.1 0.0 copy-done.2
  215.1 0.8 copy.11.affinity
  215.9 40.6 %all-to-all-done.2 = bf16[32,32,128]{2,1,0:T(8,128)(2,1)S(1)} async-done(((bf16[32,32,128]{2,1,0:T(8,128)(2,1)}), bf16[32,32,128]{2,1,0:T(8,128)(2,1)S(1)}, u32[]{:S(2)}, u32[]{:S(2)}) %all-to-all-start.2) | async-done | bytes 262176 | tf_op jit(solution)/shard_map/all_to_all | solution.py:137
  256.5 0.0 copy-start.1
  256.5 0.7 copy-done.1
  257.2 2.9 %pick.1 = bf16[256,2,128]{2,1,0:T(2,128)(2,1)} custom-call(bf16[1024,128]{1,0:T(8,128)(2,1)} %bitcast.13, s32[256,2]{1,0:T(8,128)} %copy.9.chosen, f32[256,2]{1,0:T(8,128)} %copy.11.affinity), custom_call_target="tpu_custom_call" | custom-call | tf_op jit(solution)/shard_map/pick/pallas_call | solution.py:140
Async XLA Ops:
  11.3 110.2 %all-to-all-start = ((bf16[32,32,256]{2,1,0:T(8,128)(2,1)}), bf16[32,32,256]{2,1,0:T(8,128)(2,1)S(1)}, u32[]{:S(2)}, u32[]{:S(2)}) async-start(bf16[32,32,256]{2,1,0:T(8,128)(2,1)} %bitcast.10), calls=%async_computation | async-start | bytes 1048576 | tf_op jit(solution)/shard_map/all_to_all | solution.py:103
  57.1 147.4 %all-gather.3.cloned.1.call-start = ((), (), s32[]{:S(2)}) async-start(), calls=%async_computation.3 | async-start | bytes 4718592 | tf_op jit(solution)/shard_map/all_gather | solution.py:118
  121.5 0.8 copy-start
  190.3 24.8 %copy-start.2 = (f32[256,2]{0,1:T(2,128)S(1)}, f32[256,2]{0,1:T(2,128)}, u32[]{:S(2)}) copy-start(f32[256,2]{0,1:T(2,128)} %param.11) | copy-start | bytes 6148
  190.3 13.2 %collective-permute-start = (bf16[1,32,32,256]{3,2,1,0:T(8,128)(2,1)S(1)}, bf16[1,32,32,256]{3,2,1,0:T(8,128)(2,1)S(1)}, u32[]{:S(2)}, u32[]{:S(2)}) collective-permute-start(bf16[1,32,32,256]{3,2,1,0:T(8,128)(2,1)S(1)} %bitcast.11), channel_id=1, source_target_pairs={{0,256},{256,0},{1,257},{257,1},{2,258},{258,2},{3,259},{259,3},{4... | collective-permute-start | bytes 1572872 | tf_op jit(solution)/shard_map/ppermute | solution.py:123
  209.2 47.3 %all-to-all-start.2 = ((bf16[32,32,128]{2,1,0:T(8,128)(2,1)}), bf16[32,32,128]{2,1,0:T(8,128)(2,1)S(1)}, u32[]{:S(2)}, u32[]{:S(2)}) async-start(bf16[32,32,128]{2,1,0:T(8,128)(2,1)} %bitcast.14), calls=%async_computation.2 | async-start | bytes 524288 | tf_op jit(solution)/shard_map/all_to_all | solution.py:137
  256.5 0.7 copy-start.1
Sparse Core Ops, SparseCore 0:
  122.5 29.2 all-gather.2
